TPU v7x, 256 devices: a whole 4x4x8 slice. The times are simulated.
256 devices in a mesh: rep: 2 (over z_hi), fs: 16 (over z_lo, x), tp: 8 (over y, core).
Axes of the slice: x: 4, y: 4, z: 8 (z_hi: 2, z_lo: 4; z = z_hi * 4 + z_lo), core: 2. Of those that a mesh axis runs over, the one named last changes fastest.
Arguments:
- tokens: bfloat16 [24576, 2048], P(('rep', 'fs'), 'tp'), parts along dimension 0, may hold values from -6 to 6
- mixer_gain: float32 [2048], replicated, may hold values from 0.1 to 1.9
- rec_weight: bfloat16 [2048, 2048], P('fs', 'tp'), may hold values from -0.125 to 0.125
- gate_weight: bfloat16 [2048, 2048], P('fs', 'tp'), may hold values from -0.125 to 0.125
- conv_taps: bfloat16 [4, 2048], P(None, 'tp'), may hold values from -3 to 3
- recur_map: bfloat16 [8, 256, 256], P('tp'), may hold values from -0.375 to 0.375
- input_map: bfloat16 [8, 256, 256], P('tp'), may hold values from -0.375 to 0.375
- decay_param: float32 [2048], P('tp'), may hold values from 3 to 11
- out_weight: bfloat16 [2048, 2048], P('tp', 'fs'), may hold values from -0.5 to 0.5
- mlp_gain: float32 [2048], replicated, may hold values from 0.1 to 1.9
- up_weight: bfloat16 [2048, 8192], P('fs', 'tp'), may hold values from -0.125 to 0.125
- down_weight: bfloat16 [8192, 2048], P('tp', 'fs'), may hold values from -0.0625 to 0.0625
Outputs:
- layer_out: bfloat16 [24576, 2048], P(('rep', 'fs'), 'tp'), parts along dimension 0
There are 2 independent parts, one for each index of `rep`. A program takes and returns all parts, laid end to end along the dimension named above; an argument that names none is the same for every part. Nothing has to cross between parts.
All inputs are finite; a program needn't handle non-finite values.
Results may differ from a plain program's by a relative error of at most 0.022.
Values may be sent and summed in bfloat16 or wider, within the bound.
A program may use at most 64 MiB of HBM per device.

v0:
```python
import jax
import jax.numpy as jnp
from jax import lax
from jax.sharding import PartitionSpec as P

NORM_EPSILON = 1e-06
GATE_SCALE = 8.0


def turned_gather(arrays, axis, dims):
    turned = [jnp.moveaxis(a, dim, 0) for a, dim in zip(arrays, dims)]
    widths = [t[0].size for t in turned]
    both = jnp.concatenate([t.reshape(-1, w) for t, w in zip(turned, widths)], axis=1)
    filled = lax.all_gather(both, axis, axis=0, tiled=True)
    blocks = jnp.split(filled, [sum(widths[:k]) for k in range(1, len(widths))], axis=1)
    return tuple(
        (
            jnp.moveaxis(b.reshape(-1, *t.shape[1:]), 0, dim)
            for b, t, dim in zip(blocks, turned, dims)
        )
    )


def joined_along(blocks, dim):
    blocks = jnp.moveaxis(blocks, 0, dim)
    lengths = blocks.shape
    return blocks.reshape(*lengths[:dim], lengths[dim] * lengths[dim + 1], *lengths[dim + 2 :])


def from_everyone(array, axis):
    copies = jnp.broadcast_to(array, (lax.axis_size(axis), *array.shape))
    return lax.all_to_all(copies, axis, split_axis=0, concat_axis=0, tiled=True)


def gather_directly(array, axis, dim):
    return joined_along(from_everyone(array, axis), dim)


def side_by_side(arrays, axis, dim, along):
    ends, at = ([], 0)
    for a in arrays[:-1]:
        at += a.shape[along]
        ends.append(at)
    both = jnp.concatenate(arrays, axis=along)
    return tuple(jnp.split(lax.all_gather(both, axis, axis=dim, tiled=True), ends, axis=along))


def cut_along(array, dim, count):
    lengths = array.shape
    blocks = array.reshape(*lengths[:dim], count, lengths[dim] // count, *lengths[dim + 1 :])
    return jnp.moveaxis(blocks, dim, 0)


def sent_and_summed(array, axis, dim):
    blocks = cut_along(array, dim, lax.axis_size(axis))
    arrived = lax.all_to_all(blocks, axis, split_axis=0, concat_axis=0, tiled=True)
    return arrived.astype(jnp.float32).sum(axis=0)


def rms_rows(full_rows, gain):
    widened = full_rows.astype(jnp.float32)
    inverse = lax.rsqrt(jnp.mean(widened * widened, axis=-1, keepdims=True) + NORM_EPSILON)
    return (widened * inverse * gain).astype(jnp.bfloat16)


def causal_taps(branch, conv_taps):
    widened = branch.astype(jnp.float32)
    tap_values = conv_taps.astype(jnp.float32)
    tap_count = tap_values.shape[0]
    length = widened.shape[0]
    padded = jnp.pad(widened, ((tap_count - 1, 0), (0, 0)))
    running = jnp.zeros_like(widened)
    for offset in range(tap_count):
        running = running + padded[offset : offset + length, :] * tap_values[offset]
    return running.astype(jnp.bfloat16)


def combine(earlier, latter):
    return (earlier[0] * latter[0], latter[0] * earlier[1] + latter[1])


def add_rows(operand, column_piece):
    return jnp.dot(operand, column_piece, preferred_element_type=jnp.float32)


def feature_term(whole_weight, hidden):
    return lax.dot_general(
        whole_weight, hidden, (((0,), (1,)), ((), ())), preferred_element_type=jnp.float32
    )


def recurrence(branch, gate_branch, conv_taps, recur_map, input_map, decay_param):
    length = branch.shape[0]
    block_w = recur_map.shape[1]
    conv_out = causal_taps(branch, conv_taps)
    blocks = conv_out.reshape(length, -1, block_w)
    recur_gate = jax.nn.sigmoid(
        jnp.einsum("lnc,ncd->lnd", blocks, recur_map, preferred_element_type=jnp.float32).reshape(
            length, -1
        )
    )
    input_gate = jax.nn.sigmoid(
        jnp.einsum("lnc,ncd->lnd", blocks, input_map, preferred_element_type=jnp.float32).reshape(
            length, -1
        )
    )
    log_decay = -GATE_SCALE * recur_gate * jax.nn.softplus(-decay_param)
    decay_rate = jnp.exp(log_decay)
    drive_term = jnp.sqrt(-jnp.expm1(2.0 * log_decay)) * (input_gate * conv_out.astype(jnp.float32))
    _, states = lax.associative_scan(combine, (decay_rate, drive_term), axis=0)
    return (states * jax.nn.gelu(gate_branch.astype(jnp.float32))).astype(jnp.bfloat16)


def shards(
    tokens,
    mixer_gain,
    rec_weight,
    gate_weight,
    conv_taps,
    recur_map,
    input_map,
    decay_param,
    out_weight,
    mlp_gain,
    up_weight,
    down_weight,
):
    up_whole, down_whole = turned_gather((up_weight, down_weight), "fs", (0, 1))
    full_rows = gather_directly(tokens, "tp", 1)
    normed = rms_rows(full_rows, mixer_gain)
    pieces = side_by_side((rec_weight, gate_weight), "fs", 0, 1)
    branch_sum = add_rows(normed, pieces[0])
    gate_sum = add_rows(normed, pieces[1])
    branch = branch_sum.astype(jnp.bfloat16)
    gate_branch = gate_sum.astype(jnp.bfloat16)
    mixed_out = recurrence(branch, gate_branch, conv_taps, recur_map, input_map, decay_param)
    out_whole = gather_directly(out_weight, "fs", 1)
    mixer_out = sent_and_summed(feature_term(out_whole, mixed_out).astype(jnp.bfloat16), "tp", 0).T
    middle = (tokens.astype(jnp.float32) + mixer_out).astype(jnp.bfloat16)
    middle_rows = gather_directly(middle, "tp", 1)
    normed_mlp = rms_rows(middle_rows, mlp_gain)
    lifted = jnp.dot(normed_mlp, up_whole, preferred_element_type=jnp.float32)
    squared = jnp.square(jax.nn.relu(lifted)).astype(jnp.bfloat16)
    mlp_out = sent_and_summed(feature_term(down_whole, squared).astype(jnp.bfloat16), "tp", 0).T
    return (middle.astype(jnp.float32) + mlp_out).astype(jnp.bfloat16)


def solution(mesh):
    placed = (
        P(("rep", "fs"), "tp"),
        P(),
        P("fs", "tp"),
        P("fs", "tp"),
        P(None, "tp"),
        P("tp", None, None),
        P("tp", None, None),
        P("tp"),
        P("tp", "fs"),
        P(),
        P("fs", "tp"),
        P("tp", "fs"),
    )
    return jax.shard_map(
        shards, mesh=mesh, in_specs=placed, out_specs=P(("rep", "fs"), "tp"), check_vma=False
    )
```

profile of v0, /device:TPU:1, one launch (start us, length us, event | category | flops | bytes accessed | tf_op | source)
XLA Modules:
  0.0 284.7 jit_solution(8443693442468253675)
XLA Ops:
  6.5 1.6 pad_maximum_fusion.3
  8.1 1.2 copy.24
  9.3 1.9 broadcast_in_dim.6
  11.2 6.9 %all-to-all-start = ((bf16[8,768,256]{1,2,0:T(8,128)(2,1)}), bf16[8,768,256]{1,2,0:T(8,128)(2,1)S(1)}, u32[]{:S(2)}, u32[]{:S(2)}) async-start(bf16[8,768,256]{1,2,0:T(8,128)(2,1)} %broadcast_in_dim.6), calls=%async_computation | async-start | bytes 6291456 | tf_op jit(solution)/shard_map/all_to_all | solution.py:32
  18.1 1.1 copy.27
  19.2 1.8 pad_maximum_fusion
  22.1 33.5 %all-to-all-done = bf16[8,768,256]{1,2,0:T(8,128)(2,1)S(1)} async-done(((bf16[8,768,256]{1,2,0:T(8,128)(2,1)}), bf16[8,768,256]{1,2,0:T(8,128)(2,1)S(1)}, u32[]{:S(2)}, u32[]{:S(2)}) %all-to-all-start) | async-done | bytes 3145760 | tf_op jit(solution)/shard_map/all_to_all | solution.py:32
  55.6 1.1 broadcast_in_dim.7
  56.7 7.4 %all-to-all-start.1 = ((bf16[16,256,128]{1,2,0:T(8,128)(2,1)}), bf16[16,256,128]{1,2,0:T(8,128)(2,1)}, u32[]{:S(2)}, u32[]{:S(2)}) async-start(bf16[16,256,128]{1,2,0:T(8,128)(2,1)} %broadcast_in_dim.7), calls=%async_computation.1 | async-start | bytes 2097152 | tf_op jit(solution)/shard_map/all_to_all | solution.py:32
  64.8 2.5 fusion.3
  67.3 21.2 %all-gather.3.cloned.1.call-done = bf16[2048,512]{1,0:T(8,128)(2,1)} async-done(((bf16[128,512]{1,0:T(8,128)(2,1)}), bf16[2048,512]{1,0:T(8,128)(2,1)}) %all-gather.3.cloned.1.call-update) | async-done | bytes 2097168 | tf_op jit(solution)/shard_map/all_gather | solution.py:45
  88.5 3.2 %fusion.22 = f32[768,256]{1,0:T(8,128)S(1)} fusion(bf16[768,2048]{0,1:T(8,128)(2,1)} %fusion.3, bf16[2048,512]{1,0:T(8,128)(2,1)} %all-gather.3.cloned.1.call-done), kind=kOutput, calls=%fused_computation.35 | convolution fusion | flops 805699584 | bytes 4980736 | tf_op jit(solution)/shard_map/dot_general | solution.py:83
  94.4 1.5 slice.244
  95.8 1.4 slice.248
  97.3 1.2 fusion.65
  99.6 1.0 fusion.66
  113.1 1.9 pad.77
  115.1 1.9 pad.76
  117.0 6.4 %convolution_convert_fusion = bf16[768,2048]{1,0:T(8,128)(2,1)S(1)} fusion(bf16[256,2048]{0,1:T(8,128)(2,1)} %bitcast.9, bf16[768,2048]{0,1:T(8,128)(2,1)} %fusion.3, bf16[2048,512]{1,0:T(8,128)(2,1)} %all-gather.3.cloned.1.call-done, f32[768,256]{1,0:T(8,128)} %pad.76, f32[768,256]{1,0:T(8,128)} %pad.77), kind=kOutput, calls=%fused_computation.15 | convolution fusion | flops 1614741504 | bytes 9961472 | tf_op jit(solution)/shard_map/dot_general | solution.py:87
  123.6 51.8 %all_to_all.25 = bf16[8,256,768]{1,2,0:T(8,128)(2,1)S(1)} all-to-all(bf16[8,256,768]{1,2,0:T(8,128)(2,1)S(1)} %bitcast.57), channel_id=1, replica_groups=mesh['rep'=2,'fs'=16,'tp'=8] {'tp'}, dimensions={0} | all-to-all | bytes 6291456 | tf_op jit(solution)/shard_map/all_to_all | solution.py:56
  176.9 40.5 %all_to_all.26 = bf16[8,768,256]{1,2,0:T(8,128)(2,1)S(1)} all-to-all(bf16[8,768,256]{1,2,0:T(8,128)(2,1)S(1)} %broadcast_in_dim.16), channel_id=1, replica_groups=mesh['rep'=2,'fs'=16,'tp'=8] {'tp'}, dimensions={0} | all-to-all | bytes 6291456 | tf_op jit(solution)/shard_map/all_to_all | solution.py:32
  218.1 2.5 fusion.1
  220.6 12.9 %fusion.8 = bf16[2048,768]{1,0:T(8,128)(2,1)} fusion(bf16[2048,2048]{0,1:T(8,128)(2,1)} %all-gather.5.cloned.1.call-done, bf16[768,2048]{0,1:T(8,128)(2,1)} %fusion.1), kind=kOutput, calls=%fused_computation.14 | convolution fusion | flops 6446383104 | bytes 14680064 | tf_op jit(solution)/shard_map/dot_general | solution.py:87
  233.5 42.8 %all_to_all.27 = bf16[8,256,768]{2,1,0:T(8,128)(2,1)S(1)} all-to-all(bf16[8,256,768]{2,1,0:T(8,128)(2,1)} %bitcast.59), channel_id=1, replica_groups=mesh['rep'=2,'fs'=16,'tp'=8] {'tp'}, dimensions={0} | all-to-all | bytes 6291456 | tf_op jit(solution)/shard_map/all_to_all | solution.py:56
  (150 shorter events, 21.5 us)
Async XLA Ops:
  6.5 85.6 %copy-start = (bf16[1,256,256]{2,1,0:T(8,128)(2,1)S(1)}, bf16[1,256,256]{2,1,0:T(8,128)(2,1)}, u32[]{:S(2)}) copy-start(bf16[1,256,256]{2,1,0:T(8,128)(2,1)} %param.17) | copy-start | bytes 393220
  6.5 82.0 %all-gather.3.cloned.1.call-start = ((), (), s32[]{:S(2)}) async-start(), calls=%async_computation.5 | async-start | bytes 2228224 | tf_op jit(solution)/shard_map/all_gather | solution.py:45
  11.2 9.8 %copy-start.10 = (f32[256]{0:T(256)S(1)}, f32[256]{0:T(256)}, u32[]{:S(2)}) copy-start(f32[256]{0:T(256)} %param.19) | copy-start | bytes 3076
  11.2 10.8 %copy-start.9 = (bf16[4,256]{1,0:T(4,128)(2,1)S(1)}, bf16[4,256]{1,0:T(4,128)(2,1)}, u32[]{:S(2)}) copy-start(bf16[4,256]{1,0:T(4,128)(2,1)} %param.16) | copy-start | bytes 6148
  11.2 44.4 %all-to-all-start = ((bf16[8,768,256]{1,2,0:T(8,128)(2,1)}), bf16[8,768,256]{1,2,0:T(8,128)(2,1)S(1)}, u32[]{:S(2)}, u32[]{:S(2)}) async-start(bf16[8,768,256]{1,2,0:T(8,128)(2,1)} %broadcast_in_dim.6), calls=%async_computation | async-start | bytes 6291456 | tf_op jit(solution)/shard_map/all_to_all | solution.py:32
  18.1 202.5 %all-gather.5.cloned.1.call-start = ((), (), s32[]{:S(2)}) async-start(), calls=%async_computation.6 | async-start | bytes 8912896 | tf_op jit(solution)/shard_map/all_gather | solution.py:14
  22.0 42.8 %copy-start.7 = (f32[2048]{0:T(1024)S(1)}, f32[2048]{0:T(1024)}, u32[]{:S(2)}) copy-start(f32[2048]{0:T(1024)} %param.13) | copy-start | bytes 24580
  56.7 60.3 %all-to-all-start.1 = ((bf16[16,256,128]{1,2,0:T(8,128)(2,1)}), bf16[16,256,128]{1,2,0:T(8,128)(2,1)}, u32[]{:S(2)}, u32[]{:S(2)}) async-start(bf16[16,256,128]{1,2,0:T(8,128)(2,1)} %broadcast_in_dim.7), calls=%async_computation.1 | async-start | bytes 2097152 | tf_op jit(solution)/shard_map/all_to_all | solution.py:32
  91.7 0.9 copy-start.11
  93.4 15.4 %copy-start.2 = (f32[768,256]{1,0:T(8,128)}, f32[768,256]{1,0:T(8,128)S(1)}, u32[]{:S(2)}) copy-start(f32[768,256]{1,0:T(8,128)S(1)} %fusion.17) | copy-start | bytes 2359300
  107.8 4.9 %copy-start.5 = (f32[95,256]{1,0:T(8,128)S(1)}, f32[95,256]{1,0:T(8,128)}, u32[]{:S(2)}) copy-start(f32[95,256]{1,0:T(8,128)} %slice.255) | copy-start | bytes 291844
  107.8 4.9 %copy-start.6 = (f32[95,256]{1,0:T(8,128)S(1)}, f32[95,256]{1,0:T(8,128)}, u32[]{:S(2)}) copy-start(f32[95,256]{1,0:T(8,128)} %slice.306) | copy-start | bytes 291844
  107.8 5.0 %copy-start.4 = (f32[191,256]{1,0:T(8,128)S(1)}, f32[191,256]{1,0:T(8,128)}, u32[]{:S(2)}) copy-start(f32[191,256]{1,0:T(8,128)} %slice.249) | copy-start | bytes 586756
  112.9 2.2 slice-start
  175.4 1.0 copy-start.3
  217.4 0.7 copy-start.8
  233.5 44.4 %copy-start.1 = (bf16[1,256,256]{2,1,0:T(8,128)(2,1)S(1)}, bf16[1,256,256]{2,1,0:T(8,128)(2,1)}, u32[]{:S(2)}) copy-start(bf16[1,256,256]{2,1,0:T(8,128)(2,1)} %param.17) | copy-start | bytes 393220
Sparse Core Ops, SparseCore 0:
  9.1 79.3 all-gather.2
  90.2 120.9 all-gather.4
where the time goes:
time: 286 us; the launch traced here: 285 us
  blocking collectives  135 us (47%)
  waiting for transfers between devices  54.8 us (19%)
  local copies, waits for them, and re-layouts  23.9 us (8%)
  matrix products  23.7 us (8%)
  other arithmetic  18.9 us (7%)
  starting transfers between devices  14.3 us (5%)
  between operations  14 us (5%)
    all_to_all x2, blocking collectives, sent_and_summed(): lax.all_to_all(blocks, axis, split_axis=0, concat_axis=0, tiled=True)  94.6 us
    all_to_all x1, blocking collectives, from_everyone(): return lax.all_to_all(copies, axis, split_axis=0, concat_axis=0, tiled=True)  40.5 us
    all_to_all x2, waiting for transfers between devices, from_everyone(): return lax.all_to_all(copies, axis, split_axis=0, concat_axis=0, tiled=True)  33.5 us
    all_gather x1, waiting for transfers between devices, side_by_side(): lax.all_gather(both, axis, axis=dim, tiled=True)  21.2 us
    dot_general x2, matrix products, feature_term(): lax.dot_general(whole_weight, hidden, (((0,), (1,)), ((), ())), preferred...  19.3 us
    all_to_all x2, starting transfers between devices, from_everyone(): return lax.all_to_all(copies, axis, split_axis=0, concat_axis=0, tiled=True)  14.3 us
    slice x57, local copies, waits for them, and re-layouts, recurrence(): _, states = lax.associative_scan(combine, (decay_rate, drive_term), axis=0)  12.1 us
  transfers between devices with their start and end apart: 4, of which 2 were waited for; matrix products, arithmetic and copies ran while one was open for 18% of the time, Pallas kernels for 0%

commit v1 on v0

v1 whole, which is shorter than its diff:
```python
import jax
import jax.numpy as jnp
from jax import lax
from jax.experimental import pallas as pl
from jax.experimental.pallas import tpu as pltpu
from jax.sharding import PartitionSpec as P

NORM_EPSILON = 1e-06
GATE_SCALE = 8.0
MESH = pl.DeviceIdType.MESH
F32 = jnp.float32
BF16 = jnp.bfloat16

TOK = 768
D = 2048
CH = 256
FF = 1024
CHUNKS = 4
R = TOK // CHUNKS
H = R // 2
SEGS = 8
SEG = TOK // SEGS


def send(src, dst, send_sem, recv_sem, device):
    pltpu.make_async_remote_copy(
        src_ref=src,
        dst_ref=dst,
        send_sem=send_sem,
        recv_sem=recv_sem,
        device_id=device,
        device_id_type=MESH,
    ).start()


def landed(ref, sem):
    pltpu.make_async_copy(ref, ref, sem).wait()


def minus_expm1(u):
    series = 1.0 + u * (1.0 / 8.0)
    for k in (7.0, 6.0, 5.0, 4.0, 3.0, 2.0):
        series = 1.0 + (u * (1.0 / k)) * series
    return jnp.where(u > -0.5, -u * series, 1.0 - jnp.exp(u))


def kernel(
    tokens,
    rec_shard,
    gate_shard,
    out_shard,
    up_shard,
    down_shard,
    mixer_gain,
    conv_taps,
    recur_map,
    input_map,
    decay_param,
    mlp_gain,
    result,
    w_rec,
    w_gate,
    w_out,
    w_up,
    w_down,
    tok_all,
    mid_all,
    normed,
    padded,
    gate_act,
    decay,
    drive,
    mixed,
    squared,
    part_out,
    part_own,
    from_core,
    half_sent,
    half_got,
    full_sent,
    full_got,
    local_sem,
    w_sem,
    ag_sem,
    rs_sem,
):
    rep, fs, tp = lax.axis_index("rep"), lax.axis_index("fs"), lax.axis_index("tp")
    z, x = lax.div(fs, 4), lax.rem(fs, 4)
    y, core = lax.div(tp, 2), lax.rem(tp, 2)
    other = 1 - core
    xp, xm, x2 = lax.rem(x + 1, 4), lax.rem(x + 3, 4), lax.rem(x + 2, 4)
    zp, zm, z2 = lax.rem(z + 1, 4), lax.rem(z + 3, 4), lax.rem(z + 2, 4)
    yp, ym, y2 = lax.rem(y + 1, 4), lax.rem(y + 3, 4), lax.rem(y + 2, 4)
    deep = rep * 4 + z
    deep_p, deep_m = lax.rem(deep + 1, 8), lax.rem(deep + 7, 8)
    x_up, x_down = (rep, z * 4 + xp, tp), (rep, z * 4 + xm, tp)
    z_up = (lax.div(deep_p, 4), zp * 4 + x, tp)
    z_down = (lax.div(deep_m, 4), zm * 4 + x, tp)
    y_up, y_down = (rep, fs, yp * 2 + core), (rep, fs, ym * 2 + core)
    partner = (rep, fs, y * 2 + other)

    places = (
        (tokens, tok_all.at[tp]),
        (rec_shard, w_rec.at[z, x]),
        (gate_shard, w_gate.at[z, x]),
        (out_shard, w_out.at[z, x]),
        (up_shard, w_up.at[z, x]),
        (down_shard, w_down.at[z, x]),
    )
    fills = [pltpu.make_async_copy(s, d, local_sem.at[k]) for k, (s, d) in enumerate(places)]
    for fill in fills:
        fill.start()
    barrier = pltpu.get_barrier_semaphore()
    for device in (x_up, x_down, z_up, z_down, y_up, y_down, partner):
        pl.semaphore_signal(barrier, inc=1, device_id=device, device_id_type=MESH)
    pl.semaphore_wait(barrier, 7)
    for fill in fills:
        fill.wait()

    def copies(k, w, recv, sent, *moves):
        for index, device in moves:
            ref = w.at[index]
            send(ref, ref, w_sem.at[k, sent], w_sem.at[k, recv], device)

    weights = {"rec": (0, w_rec), "gate": (1, w_gate), "out": (2, w_out), "up": (3, w_up), "down": (4, w_down)}

    def pieces(w):
        h = w.shape[2] // 2
        q = h // 2
        return pl.ds(0, h), pl.ds(h, h), pl.ds(0, q), pl.ds(q, q), pl.ds(h, q), pl.ds(h + q, q)

    def w1(name):
        k, w = weights[name]
        a, b, _, _, _, _ = pieces(w)
        copies(k, w, 0, 4, ((z, x, a), x_up), ((z, x, a), x_down), ((z, x, b), z_up), ((z, x, b), z_down))
        copies(k, w, 2, 4, ((z, x, a), z_up), ((z, x, a), z_down), ((z, x, b), x_up), ((z, x, b), x_down))

    def w2(name):
        k, w = weights[name]
        a, b, at, ab, bt, bb = pieces(w)
        landed(w.at[0, pl.ds(0, 2)], w_sem.at[k, 0])
        copies(k, w, 1, 5, ((z, xm, at), x_up), ((z, xp, ab), x_down), ((zm, x, bt), z_up), ((zp, x, bb), z_down))
        for n in (xm, xp):
            copies(k, w, 2, 4, ((z, n, a), z_up), ((z, n, a), z_down))
        for n in (zm, zp):
            copies(k, w, 2, 4, ((n, x, b), x_up), ((n, x, b), x_down))

    def w3(name):
        k, w = weights[name]
        a, b, _, _, _, _ = pieces(w)
        landed(w.at[0, 0], w_sem.at[k, 1])
        copies(k, w, 2, 5, ((z, x2, a), z_up), ((z, x2, a), z_down), ((z2, x, b), x_up), ((z2, x, b), x_down))

    def w4(name):
        k, w = weights[name]
        every = pl.ds(0, 4)
        _, _, at, ab, bt, bb = pieces(w)
        landed(w.at[pl.ds(0, 2)], w_sem.at[k, 2])
        copies(k, w, 3, 6, ((zm, every, at), z_up), ((zp, every, ab), z_down), ((every, xm, bt), x_up), ((every, xp, bb), x_down))

    def w5(name):
        k, w = weights[name]
        landed(w.at[0], w_sem.at[k, 3])

    def w_drain():
        for k, w in weights.values():
            landed(w.at[pl.ds(0, 2)], w_sem.at[k, 4])
            landed(w.at[0, pl.ds(0, 3)], w_sem.at[k, 5])
            landed(w.at[0], w_sem.at[k, 6])

    jp, jm, j2 = yp * 2 + core, ym * 2 + core, y2 * 2 + core

    def ag(k, buf, first, count):
        rows, top, bottom = pl.ds(first, count), pl.ds(first, count // 2), pl.ds(first + count // 2, count // 2)
        sem = lambda n: ag_sem.at[k, n]
        move = lambda index, recv, device: send(buf.at[index], buf.at[index], sem(3), sem(recv), device)

        def one():
            move((tp, rows), 0, y_up)
            move((tp, rows), 0, y_down)
            move((tp, rows), 2, partner)

        def two():
            landed(buf.at[pl.ds(0, 2), rows], sem(0))
            move((jm, top), 1, y_up)
            move((jp, bottom), 1, y_down)
            move((jm, rows), 2, partner)
            move((jp, rows), 2, partner)

        def three():
            landed(buf.at[0, rows], sem(1))
            move((j2, rows), 2, partner)

        def four():
            landed(buf.at[pl.ds(0, 4), rows], sem(2))

        def drain():
            landed(buf.at[pl.ds(0, 7), rows], sem(3))

        return one, two, three, four, drain

    top, bottom = pl.ds(0, H), pl.ds(H, H)

    def rs(k):
        sem = lambda n: rs_sem.at[k, n]
        both = lambda n: part_own[k, n].astype(F32) + from_core[k, n].astype(F32)

        def zero(term):
            for n in range(4):
                part_out[k, n] = term(n, other).astype(BF16)
            send(part_out.at[k], from_core.at[k], sem(3), sem(0), partner)
            for n in range(4):
                part_own[k, n] = term(n, core).astype(BF16)

        def one():
            landed(from_core.at[k], sem(0))
            half_sent[k] = both(y2).astype(BF16)
            send(half_sent.at[k, top], half_got.at[k, top], sem(4), sem(1), y_up)
            send(half_sent.at[k, bottom], half_got.at[k, bottom], sem(4), sem(1), y_down)

        def two():
            landed(half_got.at[k], sem(1))
            up, down = both(yp), both(ym)
            got = half_got[k].astype(F32)
            full_sent[k, 0] = jnp.concatenate([up[:H] + got[:H], up[H:]], axis=0).astype(BF16)
            send(full_sent.at[k, 0], full_got.at[k, 0], sem(5), sem(2), y_up)
            full_sent[k, 1] = jnp.concatenate([down[:H], down[H:] + got[H:]], axis=0).astype(BF16)
            send(full_sent.at[k, 1], full_got.at[k, 1], sem(5), sem(2), y_down)

        def three():
            landed(full_got.at[k], sem(2))
            return both(y) + (full_got[k, 0].astype(F32) + full_got[k, 1].astype(F32))

        def drain():
            landed(part_out.at[k], sem(3))
            landed(half_sent.at[k], sem(4))
            landed(full_sent.at[k], sem(5))

        return zero, one, two, three, drain

    def norm(buf, gain, first, count):
        step = 32

        def body(i, _):
            rows = pl.ds(pl.multiple_of(first + i * step, step), step)
            total = jnp.zeros((step, CH), F32)
            for j in range(8):
                v = buf[j, rows, :].astype(F32)
                total = total + v * v
            inverse = lax.rsqrt(jnp.sum(total, axis=-1, keepdims=True) * (1.0 / D) + NORM_EPSILON)
            for j in range(8):
                v = buf[j, rows, :].astype(F32)
                normed[rows, CH * j : CH * (j + 1)] = (v * inverse * gain[:, CH * j : CH * (j + 1)]).astype(BF16)
            return 0

        lax.fori_loop(0, count // step, body, 0)

    def project(m, _):
        rows = pl.ds(pl.multiple_of(m * 256, 256), 256)
        lhs = normed[rows, :]
        branch = jnp.dot(lhs, w_rec[...].reshape(D, CH), preferred_element_type=F32)
        padded[pl.ds(pl.multiple_of(m * 256 + 8, 8), 256), :] = branch.astype(BF16).astype(F32)
        gate = jnp.dot(lhs, w_gate[...].reshape(D, CH), preferred_element_type=F32)
        gate_act[rows, :] = jax.nn.gelu(gate.astype(BF16).astype(F32), approximate=True)
        return 0

    def gates(m, _):
        rows = pl.ds(pl.multiple_of(m * 128, 128), 128)
        window = padded[pl.ds(pl.multiple_of(m * 128, 128), 136), :]
        running = jnp.zeros((128, CH), F32)
        for k in range(4):
            running = running + window[5 + k : 133 + k] * conv_taps[k : k + 1, :].astype(F32)
        conv = running.astype(BF16)
        recur = jax.nn.sigmoid(jnp.dot(conv, recur_map[0], preferred_element_type=F32))
        enter = jax.nn.sigmoid(jnp.dot(conv, input_map[0], preferred_element_type=F32))
        p = -decay_param[...]
        softplus = jnp.maximum(p, 0.0) + jnp.log1p(jnp.exp(-jnp.abs(p)))
        log_decay = -GATE_SCALE * recur * softplus
        a = jnp.exp(log_decay)
        s = jnp.sqrt(minus_expm1(2.0 * log_decay)) * (enter * conv.astype(F32))
        for half in range(2):
            cols = slice(128 * half, 128 * (half + 1))
            decay[half, rows, :] = a[:, cols]
            drive[half, rows, :] = s[:, cols]
        return 0

    def scan():
        def body(k, carry):
            new = []
            for half in range(2):
                h, p = carry[half]
                at = pl.ds(k, SEGS, SEG)
                a = decay[half, at, :]
                h = a * h + drive[half, at, :]
                p = a * p
                drive[half, at, :] = h
                decay[half, at, :] = p
                new.append((h, p))
            return tuple(new)

        start = (jnp.zeros((SEGS, 128), F32), jnp.ones((SEGS, 128), F32))
        lax.fori_loop(0, SEG, body, (start, start), unroll=8)
        for half in range(2):
            cols = slice(128 * half, 128 * (half + 1))
            carry = jnp.zeros((1, 128), F32)
            for n in range(SEGS):
                rows = slice(SEG * n, SEG * (n + 1))
                state = drive[half, rows, :] + decay[half, rows, :] * carry
                carry = state[SEG - 1 : SEG]
                mixed[rows, cols] = (state * gate_act[rows, cols]).astype(BF16)

    def out_term(c):
        lhs = mixed[pl.ds(c * R, R), :]

        def term(n, side):
            rhs = jnp.concatenate([w_out[n, 2 * side], w_out[n, 2 * side + 1]], axis=1)
            return jnp.dot(lhs, rhs, preferred_element_type=F32)

        return term

    def lift(c):
        lhs = normed[pl.ds(c * R, R), :]
        for n in range(FF // 256):
            rhs = w_up[:, :, :, 256 * n : 256 * (n + 1)].reshape(D, 256)
            lifted = jnp.maximum(jnp.dot(lhs, rhs, preferred_element_type=F32), 0.0)
            squared[:, 256 * n : 256 * (n + 1)] = (lifted * lifted).astype(BF16)

    def down_term(n, side):
        rhs = jnp.concatenate([w_down[n, 2 * side], w_down[n, 2 * side + 1]], axis=1)
        return jnp.dot(squared[...], rhs, preferred_element_type=F32)

    t1, t2, t3, t4, t_drain = ag(0, tok_all, 0, TOK)
    w1("rec")
    w1("gate")
    t1()
    w2("rec")
    w2("gate")
    w1("out")
    t2()
    w3("rec")
    w3("gate")
    w2("out")
    w4("rec")
    w4("gate")
    t3()
    w3("out")
    w1("up")
    t4()
    norm(tok_all, mixer_gain, 0, TOK)
    w4("out")
    padded[pl.ds(0, 8), :] = jnp.zeros((8, CH), F32)
    w5("rec")
    w5("gate")
    w2("up")
    lax.fori_loop(0, TOK // 256, project, 0)
    w3("up")
    w1("down")
    lax.fori_loop(0, TOK // 128, gates, 0)
    scan()
    w5("out")
    w4("up")
    w2("down")

    mixer = [rs(c) for c in range(CHUNKS)]
    spread = [ag(1 + c, mid_all, c * R, R) for c in range(CHUNKS)]
    mlp = [rs(CHUNKS + c) for c in range(CHUNKS)]

    def middle(c):
        rows = pl.ds(c * R, R)
        total = mixer[c][3]()
        mid_all[tp, rows, :] = (tok_all[tp, rows, :].astype(F32) + total).astype(BF16)
        spread[c][0]()

    def feed(c):
        spread[c][3]()
        norm(mid_all, mlp_gain, c * R, R)
        if c == 0:
            w5("up")
        lift(c)
        if c == 0:
            w5("down")
        mlp[c][0](down_term)

    def finish(c):
        rows = pl.ds(c * R, R)
        result[rows, :] = (mid_all[tp, rows, :].astype(F32) + mlp[c][3]()).astype(BF16)

    stages = (
        lambda c: mixer[c][0](out_term(c)),
        lambda c: mixer[c][1](),
        lambda c: mixer[c][2](),
        middle,
        lambda c: spread[c][1](),
        lambda c: spread[c][2](),
        feed,
        lambda c: mlp[c][1](),
        lambda c: mlp[c][2](),
        finish,
    )
    for t in range(CHUNKS + len(stages) - 1):
        if t == 3:
            w3("down")
        if t == 5:
            w4("down")
        for n, stage in enumerate(stages):
            if 0 <= t - n < CHUNKS:
                stage(t - n)

    w_drain()
    t_drain()
    for group in (mixer, spread, mlp):
        for g in group:
            g[4]()


def shards(
    tokens,
    mixer_gain,
    rec_weight,
    gate_weight,
    conv_taps,
    recur_map,
    input_map,
    decay_param,
    out_weight,
    mlp_gain,
    up_weight,
    down_weight,
):
    hbm = pl.BlockSpec(memory_space=pl.ANY)
    vmem = pl.BlockSpec(memory_space=pltpu.VMEM)
    sums = 2 * CHUNKS
    return pl.pallas_call(
        kernel,
        out_shape=jax.ShapeDtypeStruct((TOK, CH), BF16),
        in_specs=[hbm] * 6 + [vmem] * 6,
        out_specs=vmem,
        scratch_shapes=[
            pltpu.VMEM((4, 4, D // 16, CH), BF16),
            pltpu.VMEM((4, 4, D // 16, CH), BF16),
            pltpu.VMEM((4, 4, CH, D // 16), BF16),
            pltpu.VMEM((4, 4, D // 16, FF), BF16),
            pltpu.VMEM((4, 4, FF, D // 16), BF16),
            pltpu.VMEM((8, TOK, CH), BF16),
            pltpu.VMEM((8, TOK, CH), BF16),
            pltpu.VMEM((TOK, D), BF16),
            pltpu.VMEM((TOK + 8, CH), F32),
            pltpu.VMEM((TOK, CH), F32),
            pltpu.VMEM((2, TOK, 128), F32),
            pltpu.VMEM((2, TOK, 128), F32),
            pltpu.VMEM((TOK, CH), BF16),
            pltpu.VMEM((R, FF), BF16),
            pltpu.VMEM((sums, 4, R, CH), BF16),
            pltpu.VMEM((sums, 4, R, CH), BF16),
            pltpu.VMEM((sums, 4, R, CH), BF16),
            pltpu.VMEM((sums, R, CH), BF16),
            pltpu.VMEM((sums, R, CH), BF16),
            pltpu.VMEM((sums, 2, R, CH), BF16),
            pltpu.VMEM((sums, 2, R, CH), BF16),
            pltpu.SemaphoreType.DMA((6,)),
            pltpu.SemaphoreType.DMA((5, 7)),
            pltpu.SemaphoreType.DMA((1 + CHUNKS, 4)),
            pltpu.SemaphoreType.DMA((sums, 6)),
        ],
        compiler_params=pltpu.CompilerParams(
            collective_id=0, has_side_effects=True, vmem_limit_bytes=60 * 1024 * 1024
        ),
    )(
        tokens,
        rec_weight,
        gate_weight,
        out_weight,
        up_weight,
        down_weight,
        mixer_gain.reshape(1, D),
        conv_taps,
        recur_map,
        input_map,
        decay_param.reshape(1, CH),
        mlp_gain.reshape(1, D),
    )


def solution(mesh):
    placed = (
        P(("rep", "fs"), "tp"),
        P(),
        P("fs", "tp"),
        P("fs", "tp"),
        P(None, "tp"),
        P("tp", None, None),
        P("tp", None, None),
        P("tp"),
        P("tp", "fs"),
        P(),
        P("fs", "tp"),
        P("tp", "fs"),
    )
    return jax.shard_map(
        shards, mesh=mesh, in_specs=placed, out_specs=P(("rep", "fs"), "tp"), check_vma=False
    )
```

time: 286 us -> 106 us (0.37)
  blocking collectives: 135 us -> 0 us
  Pallas kernels: 0 us -> 104 us
  waiting for transfers between devices: 54.8 us -> 0 us
  matrix products: 23.7 us -> 0 us
  local copies, waits for them, and re-layouts: 23.9 us -> 1.77 us
  other arithmetic: 18.9 us -> 0 us
  starting transfers between devices: 14.3 us -> 0 us
  between operations: 14 us -> 0.01 us
    all_to_all x3 -> x0, blocking collectives: 135 us -> none  [the longest x2 94.6 us: sent_and_summed(): lax.all_to_all(blocks, axis, split_axis=0, concat_axis=0, tiled=True)]
    pallas_call x0 -> x1, Pallas kernels: none -> 104 us  [shards(): pl.pallas_call(kernel, out_shape=jax.ShapeDtypeStruct((TOK, CH), BF16), i...]
    all_to_all x2 -> x0, waiting for transfers between devices: 33.5 us -> none  [from_everyone(): return lax.all_to_all(copies, axis, split_axis=0, concat_axis=0, tiled=True)]
    dot_general x5 -> x0, matrix products: 23.7 us -> none  [the longest x2 19.3 us: feature_term(): lax.dot_general(whole_weight, hidden, (((0,), (1,)), ((), ())), preferred...]
    all_gather x2 -> x0, waiting for transfers between devices: 21.3 us -> none  [the longest x1 21.2 us: side_by_side(): lax.all_gather(both, axis, axis=dim, tiled=True)]
    all_to_all x2 -> x0, starting transfers between devices: 14.3 us -> none  [from_everyone(): return lax.all_to_all(copies, axis, split_axis=0, concat_axis=0, tiled=True)]
    slice x58 -> x0, local copies, waits for them, and re-layouts: 12.2 us -> none  [the longest x57 12.1 us: recurrence(): _, states = lax.associative_scan(combine, (decay_rate, drive_term), axis=0)]
    convert_element_type x5 -> x0, other arithmetic: 6.24 us -> none  [the longest x2 4.96 us: rms_rows(): return (widened * inverse * gain).astype(jnp.bfloat16)]
  transfers between devices with their start and end apart: 4 -> 0, of which waited for: 2 -> 0; matrix products, arithmetic and copies ran while one was open for 18% -> 0% of each run, Pallas kernels for 0% -> 0%
where the time goes in v1:
time: 106 us
  Pallas kernels  104 us (98%)
  local copies, waits for them, and re-layouts  1.77 us (2%)
    pallas_call x1, Pallas kernels, shards(): pl.pallas_call(kernel, out_shape=jax.ShapeDtypeStruct((TOK, CH), BF16), i...  104 us

profile of v1, /device:TPU:1, one launch (start us, length us, event | category | flops | bytes accessed | tf_op | source)
XLA Modules:
  0.0 105.7 jit_solution(14069942296131488788)
XLA Ops:
  0.0 103.9 %shard_map.118 = bf16[768,256]{1,0:T(8,128)(2,1)} custom-call(bf16[768,256]{1,0:T(8,128)(2,1)} %tokens.1, bf16[128,256]{1,0:T(8,128)(2,1)} %rec_shard.1, bf16[128,256]{1,0:T(8,128)(2,1)} %gate_shard.1, bf16[256,128]{1,0:T(8,128)(2,1)} %out_shard.1, bf16[128,1024]{1,0:T(8,128)(2,1)} %up_shard.1, bf16[1024,128]{1,0:T(8,128)(2,1)} %down_shard.1, ...), custom_call_target="tpu_custom_call" | custom-call | tf_op jit(solution)/shard_map/pallas_call | solution.py:433
  103.9 1.8 %copy.14 = bf16[768,256]{1,0:T(8,128)(2,1)} copy(bf16[768,256]{1,0:T(8,128)(2,1)} %shard_map.118) | data formatting | bytes 786432

commit v2 on v1

v2 whole, which is shorter than its diff:
```python
import jax
import jax.numpy as jnp
from jax import lax
from jax.experimental import pallas as pl
from jax.experimental.pallas import tpu as pltpu
from jax.sharding import PartitionSpec as P

NORM_EPSILON = 1e-06
GATE_SCALE = 8.0
MESH = pl.DeviceIdType.MESH
F32 = jnp.float32
BF16 = jnp.bfloat16

TOK = 768
D = 2048
CH = 256
FF = 1024
CHUNKS = 4
PARTS = 3
PART = TOK // PARTS
R = TOK // CHUNKS
H = R // 2
SEGS = 16
SEG = PART // SEGS


def send(src, dst, send_sem, recv_sem, device):
    pltpu.make_async_remote_copy(
        src_ref=src,
        dst_ref=dst,
        send_sem=send_sem,
        recv_sem=recv_sem,
        device_id=device,
        device_id_type=MESH,
    ).start()


def landed(ref, sem):
    with jax.named_scope("wait"):
        pltpu.make_async_copy(ref, ref, sem).wait()


def minus_expm1(u):
    series = 1.0 + u * (1.0 / 8.0)
    for k in (7.0, 6.0, 5.0, 4.0, 3.0, 2.0):
        series = 1.0 + (u * (1.0 / k)) * series
    return jnp.where(u > -0.5, -u * series, 1.0 - jnp.exp(u))


def kernel(
    tokens,
    rec_shard,
    gate_shard,
    out_shard,
    up_shard,
    down_shard,
    mixer_gain_in,
    conv_taps_in,
    recur_map_in,
    input_map_in,
    decay_param_in,
    mlp_gain_in,
    result,
    mixer_gain,
    conv_taps,
    recur_map,
    input_map,
    decay_param,
    mlp_gain,
    w_rec,
    w_gate,
    w_out,
    w_up,
    w_d0,
    w_d1,
    down_raw,
    w_dn,
    tok_all,
    mid_all,
    normed,
    padded,
    gate_act,
    decay,
    drive,
    mixed,
    squared,
    first_sum,
    m_part,
    m_core,
    m_half_sent,
    m_half_got,
    m_full_sent,
    m_full_got,
    f_part,
    f_core,
    f_half_sent,
    f_half_got,
    f_full_sent,
    f_full_got,
    local_sem,
    w_sem,
    w_sent,
    ag_sem,
    ag_sent,
    m_sem,
    m_sent,
    f_sem,
    f_sent,
):
    rep, fs, tp = lax.axis_index("rep"), lax.axis_index("fs"), lax.axis_index("tp")
    z, x = lax.div(fs, 4), lax.rem(fs, 4)
    y, core = lax.div(tp, 2), lax.rem(tp, 2)
    other = 1 - core
    xp, xm, x2 = lax.rem(x + 1, 4), lax.rem(x + 3, 4), lax.rem(x + 2, 4)
    zp, zm, z2 = lax.rem(z + 1, 4), lax.rem(z + 3, 4), lax.rem(z + 2, 4)
    yp, ym, y2 = lax.rem(y + 1, 4), lax.rem(y + 3, 4), lax.rem(y + 2, 4)
    deep = rep * 4 + z
    deep_p, deep_m = lax.rem(deep + 1, 8), lax.rem(deep + 7, 8)
    x_up, x_down = (rep, z * 4 + xp, tp), (rep, z * 4 + xm, tp)
    z_up = (lax.div(deep_p, 4), zp * 4 + x, tp)
    z_down = (lax.div(deep_m, 4), zm * 4 + x, tp)
    y_up, y_down = (rep, fs, yp * 2 + core), (rep, fs, ym * 2 + core)
    partner = (rep, fs, y * 2 + other)

    places = (
        (tokens, tok_all.at[tp]),
        (rec_shard, w_rec.at[z * 4 + x]),
        (gate_shard, w_gate.at[z * 4 + x]),
        (out_shard, w_out.at[z * 4 + x]),
        (up_shard, w_up.at[z * 4 + x]),
        (down_shard, down_raw),
        (mixer_gain_in, mixer_gain),
        (conv_taps_in, conv_taps),
        (recur_map_in, recur_map),
        (input_map_in, input_map),
        (decay_param_in, decay_param),
        (mlp_gain_in, mlp_gain),
    )
    fills = [pltpu.make_async_copy(s, d, local_sem.at[k]) for k, (s, d) in enumerate(places)]
    for fill in fills:
        fill.start()
    barrier = pltpu.get_barrier_semaphore()
    with jax.named_scope("barrier"):
        for device in (x_up, x_down, z_up, z_down, y_up, y_down, partner):
            pl.semaphore_signal(barrier, inc=1, device_id=device, device_id_type=MESH)
        pl.semaphore_wait(barrier, 7)
    for fill in fills:
        fill.wait()

    def copies(k, w, recv, *moves):
        for (i, j, rows), device in moves:
            ref = w.at[i * 4 + j, rows]
            send(ref, ref, w_sent.at[k], w_sem.at[k, recv], device)

    weights = {"rec": (0, w_rec), "gate": (1, w_gate), "out": (2, w_out), "up": (3, w_up), "d0": (4, w_d0), "d1": (5, w_d1)}

    def pieces(w):
        h = w.shape[1] // 2
        q = h // 2
        return pl.ds(0, h), pl.ds(h, h), pl.ds(0, q), pl.ds(q, q), pl.ds(h, q), pl.ds(h + q, q)

    def w1(name):
        k, w = weights[name]
        a, b, _, _, _, _ = pieces(w)
        copies(k, w, 0, ((z, x, a), x_up), ((z, x, a), x_down), ((z, x, b), z_up), ((z, x, b), z_down))
        copies(k, w, 2, ((z, x, a), z_up), ((z, x, a), z_down), ((z, x, b), x_up), ((z, x, b), x_down))

    def w2(name):
        k, w = weights[name]
        a, b, at, ab, bt, bb = pieces(w)
        landed(w.at[pl.ds(0, 2)], w_sem.at[k, 0])
        copies(k, w, 1, ((z, xm, at), x_up), ((z, xp, ab), x_down), ((zm, x, bt), z_up), ((zp, x, bb), z_down))
        for n in (xm, xp):
            copies(k, w, 2, ((z, n, a), z_up), ((z, n, a), z_down))
        for n in (zm, zp):
            copies(k, w, 2, ((n, x, b), x_up), ((n, x, b), x_down))

    def w3(name):
        k, w = weights[name]
        a, b, _, _, _, _ = pieces(w)
        landed(w.at[0], w_sem.at[k, 1])
        copies(k, w, 4, ((z, x2, a), z_up), ((z, x2, a), z_down), ((z2, x, b), x_up), ((z2, x, b), x_down))

    def w4(name):
        k, w = weights[name]
        _, _, at, ab, bt, bb = pieces(w)
        landed(w.at[pl.ds(0, 6)], w_sem.at[k, 2])
        for n in (x, xm, xp):
            copies(k, w, 3, ((zm, n, at), z_up), ((zp, n, ab), z_down))
        for n in (z, zm, zp):
            copies(k, w, 3, ((n, xm, bt), x_up), ((n, xp, bb), x_down))

    def w6(name):
        k, w = weights[name]
        _, _, at, ab, bt, bb = pieces(w)
        landed(w.at[pl.ds(0, 2)], w_sem.at[k, 4])
        copies(k, w, 3, ((zm, x2, at), z_up), ((zp, x2, ab), z_down), ((z2, xm, bt), x_up), ((z2, xp, bb), x_down))

    def w5(name):
        k, w = weights[name]
        landed(w.at[pl.ds(0, 4)], w_sem.at[k, 3])

    def w_drain():
        for k, w in weights.values():
            landed(w.at[pl.ds(0, 15)], w_sent.at[k])

    jp, jm, j2 = yp * 2 + core, ym * 2 + core, y2 * 2 + core

    def ag(k, buf, first, count, sent):
        rows, top, bottom = pl.ds(first, count), pl.ds(first, count // 2), pl.ds(first + count // 2, count // 2)
        sem = lambda n: ag_sem.at[k, n]
        move = lambda index, recv, device: send(buf.at[index], buf.at[index], sent, sem(recv), device)

        def one():
            move((tp, rows), 0, y_up)
            move((tp, rows), 0, y_down)
            move((tp, rows), 2, partner)

        def two():
            landed(buf.at[pl.ds(0, 2), rows], sem(0))
            move((jm, top), 1, y_up)
            move((jp, bottom), 1, y_down)
            move((jm, rows), 2, partner)
            move((jp, rows), 2, partner)

        def three():
            landed(buf.at[0, rows], sem(1))
            move((j2, rows), 2, partner)

        def four():
            landed(buf.at[pl.ds(0, 4), rows], sem(2))

        return one, two, three, four

    top, bottom = pl.ds(0, H), pl.ds(H, H)

    def rs(k, part, from_core, half_sent, half_got, full_sent, full_got, sems, sent):
        sem = lambda n: sems.at[k, n]
        both = lambda n: part[k, core, n].astype(F32) + from_core[k, n].astype(F32)

        def start():
            send(part.at[k, other], from_core.at[k], sent.at[0], sem(0), partner)

        def one():
            landed(from_core.at[k], sem(0))
            half_sent[k] = both(y2).astype(BF16)
            send(half_sent.at[k, top], half_got.at[k, top], sent.at[1], sem(1), y_up)
            send(half_sent.at[k, bottom], half_got.at[k, bottom], sent.at[1], sem(1), y_down)

        def two():
            landed(half_got.at[k], sem(1))
            up, down = both(yp), both(ym)
            got = half_got[k].astype(F32)
            full_sent[k, 0] = jnp.concatenate([up[:H] + got[:H], up[H:]], axis=0).astype(BF16)
            send(full_sent.at[k, 0], full_got.at[k, 0], sent.at[2], sem(2), y_up)
            full_sent[k, 1] = jnp.concatenate([down[:H], down[H:] + got[H:]], axis=0).astype(BF16)
            send(full_sent.at[k, 1], full_got.at[k, 1], sent.at[2], sem(2), y_down)

        def three():
            landed(full_got.at[k], sem(2))
            return both(y) + (full_got[k, 0].astype(F32) + full_got[k, 1].astype(F32))

        return start, one, two, three

    def norm(buf, gain, first, count):
        step = 64

        def body(i, _):
            rows = pl.ds(pl.multiple_of(first + i * step, step), step)
            total = jnp.zeros((step, CH), F32)
            for j in range(8):
                v = buf[j, rows, :].astype(F32)
                total = total + v * v
            inverse = lax.rsqrt(jnp.sum(total, axis=-1, keepdims=True) * (1.0 / D) + NORM_EPSILON)
            for j in range(8):
                v = buf[j, rows, :].astype(F32)
                normed[rows, CH * j : CH * (j + 1)] = (v * inverse * gain[:, CH * j : CH * (j + 1)]).astype(BF16)
            return 0

        lax.fori_loop(0, count // step, body, 0)

    def project(m):
        rows = pl.ds(m * 256, 256)
        lhs = normed[rows, :]
        branch = jnp.dot(lhs, w_rec[...].reshape(D, CH), preferred_element_type=F32)
        padded[pl.ds(m * 256 + 8, 256), :] = branch.astype(BF16).astype(F32)
        gate = jnp.dot(lhs, w_gate[...].reshape(D, CH), preferred_element_type=F32)
        gate_act[rows, :] = jax.nn.gelu(gate.astype(BF16).astype(F32), approximate=True)

    def gates(m, _):
        rows = pl.ds(pl.multiple_of(m * 128, 128), 128)
        window = padded[pl.ds(pl.multiple_of(m * 128, 128), 136), :]
        running = jnp.zeros((128, CH), F32)
        for k in range(4):
            running = running + window[5 + k : 133 + k] * conv_taps[k : k + 1, :].astype(F32)
        conv = running.astype(BF16)
        recur = jax.nn.sigmoid(jnp.dot(conv, recur_map[0], preferred_element_type=F32))
        enter = jax.nn.sigmoid(jnp.dot(conv, input_map[0], preferred_element_type=F32))
        p = -decay_param[...]
        softplus = jnp.maximum(p, 0.0) + jnp.log1p(jnp.exp(-jnp.abs(p)))
        log_decay = -GATE_SCALE * recur * softplus
        a = jnp.exp(log_decay)
        s = jnp.sqrt(minus_expm1(2.0 * log_decay)) * (enter * conv.astype(F32))
        for half in range(2):
            cols = slice(128 * half, 128 * (half + 1))
            decay[half, rows, :] = a[:, cols]
            drive[half, rows, :] = s[:, cols]
        return 0

    carries = [jnp.zeros((1, 128), F32)] * 2

    def scan(m):
        base = m * PART

        def body(k, carry):
            new = []
            for half in range(2):
                h, p = carry[half]
                at = pl.ds(base + k, SEGS, SEG)
                a = decay[half, at, :]
                h = a * h + drive[half, at, :]
                p = a * p
                drive[half, at, :] = h
                decay[half, at, :] = p
                new.append((h, p))
            return tuple(new)

        first = (jnp.zeros((SEGS, 128), F32), jnp.ones((SEGS, 128), F32))
        lax.fori_loop(0, SEG, body, (first, first), unroll=8)
        for half in range(2):
            cols = slice(128 * half, 128 * (half + 1))
            carry = carries[half]
            for n in range(SEGS):
                rows = slice(base + SEG * n, base + SEG * (n + 1))
                state = drive[half, rows, :] + decay[half, rows, :] * carry
                carry = state[SEG - 1 : SEG]
                mixed[rows, cols] = (state * gate_act[rows, cols]).astype(BF16)
            carries[half] = carry

    def out_product(c):
        lhs = mixed[pl.ds(c * R, R), :]
        for side in (other, core):
            for n in range(4):
                rhs = jnp.concatenate([w_out[4 * n + 2 * side], w_out[4 * n + 2 * side + 1]], axis=1)
                m_part[c, side, n] = jnp.dot(lhs, rhs, preferred_element_type=F32).astype(BF16)
            if side is other:
                mixer[c][0]()

    def lift(c):
        lhs = normed[pl.ds(c * R, R), :]
        for n in range(FF // 256):
            rhs = w_up[:, :, 256 * n : 256 * (n + 1)].reshape(D, 256)
            lifted = jnp.maximum(jnp.dot(lhs, rhs, preferred_element_type=F32), 0.0)
            squared[pl.ds(c * R, R), 256 * n : 256 * (n + 1)] = (lifted * lifted).astype(BF16)

    def low_lanes(shape):
        return lax.broadcasted_iota(jnp.int32, shape, 1) < 64

    def pack():
        step = 128

        def body(i, _):
            upper = down_raw[pl.ds(pl.multiple_of(i * step, step), step), :].astype(F32)
            lower = down_raw[pl.ds(pl.multiple_of(i * step + FF // 2, step), step), :].astype(F32)
            low = low_lanes((step, 128))
            rows = pl.ds(pl.multiple_of(i * step, step), step)
            w_d0[z * 4 + x, rows, :] = jnp.where(low, upper, pltpu.roll(lower, 64, 1)).astype(BF16)
            w_d1[z * 4 + x, rows, :] = jnp.where(low, pltpu.roll(upper, 64, 1), lower).astype(BF16)
            return 0

        lax.fori_loop(0, FF // 2 // step, body, 0)

    def unpack_rows(g, n, side, first):
        w, step = (w_d0, w_d1)[g], FF // 4
        low = low_lanes((128, 128))
        cols = pl.ds(pl.multiple_of(128 * side, 128), 128)
        for k in range(step // 128):
            left = w[4 * n + 2 * side, pl.ds(first + 128 * k, 128), :].astype(F32)
            right = w[4 * n + 2 * side + 1, pl.ds(first + 128 * k, 128), :].astype(F32)
            w_dn[g, n, pl.ds(first + 128 * k, 128), cols] = jnp.where(low, left, pltpu.roll(right, 64, 1)).astype(BF16)
            w_dn[g, n, pl.ds(first + FF // 2 + 128 * k, 128), cols] = jnp.where(low, pltpu.roll(left, 64, 1), right).astype(BF16)

    def unpack(g, late):
        pair = lax.div(x, 2)

        def body(i, _):
            if late:
                unpack_rows(g, i, 1 - pair, FF // 4)
            else:
                unpack_rows(g, i, pair, FF // 4)
            return 0

        lax.fori_loop(0, 4, body, 0)
        for n in (z2,) if late else (z, zm, zp):
            for side in range(2):
                unpack_rows(g, n, side, 0)

    def down_product(g, c):
        k = g * CHUNKS + c
        lhs = squared[pl.ds(c * R, R), :]
        for n in range(4):
            product = jnp.dot(lhs, w_dn[g, n], preferred_element_type=F32).astype(BF16)
            f_part[k, 0, n] = product[:, :128]
            f_part[k, 1, n] = product[:, 128:]
        mlp[k][0]()

    parts = [ag(n, tok_all, n * PART, PART, ag_sent.at[0]) for n in range(PARTS)]
    spread = [ag(PARTS + c, mid_all, c * R, R, ag_sent.at[1]) for c in range(CHUNKS)]
    m_bufs = (m_part, m_core, m_half_sent, m_half_got, m_full_sent, m_full_got, m_sem, m_sent)
    f_bufs = (f_part, f_core, f_half_sent, f_half_got, f_full_sent, f_full_got, f_sem, f_sent)
    mixer = [rs(c, *m_bufs) for c in range(CHUNKS)]
    mlp = [rs(k, *f_bufs) for k in range(2 * CHUNKS)]

    def middle(c):
        rows = pl.ds(c * R, R)
        total = mixer[c][3]()
        mid_all[tp, rows, :] = (tok_all[tp, rows, :].astype(F32) + total).astype(BF16)
        spread[c][0]()

    def feed(c):
        spread[c][3]()
        norm(mid_all, mlp_gain, c * R, R)
        lift(c)

    def finish(g, c):
        rows = pl.ds(c * R, R)
        total = mlp[g * CHUNKS + c][3]()
        if g == 0:
            first_sum[rows, :] = total
        else:
            early, low = first_sum[rows, :], low_lanes((R, 128))
            left = jnp.where(low, early, pltpu.roll(total, 64, 1))
            right = jnp.where(low, pltpu.roll(early, 64, 1), total)
            result[rows, :128] = (mid_all[tp, rows, :128].astype(F32) + left).astype(BF16)
            result[rows, 128:] = (mid_all[tp, rows, 128:].astype(F32) + right).astype(BF16)

    w_steps = {"w1": w1, "w2": w2, "w3": w3, "w4": w4, "w5": w5, "w6": w6}

    def part_start(m):
        norm(tok_all, mixer_gain, m * PART, PART)
        if m == 0:
            padded[pl.ds(0, 8), :] = jnp.zeros((8, CH), F32)
            w5("rec")
            w5("gate")
        project(m)

    def part_end(m):
        lax.fori_loop(2 * m, 2 * m + 2, gates, 0)
        scan(m)

    m_steps = (
        out_product,
        lambda c: mixer[c][1](),
        lambda c: mixer[c][2](),
        middle,
        lambda c: spread[c][1](),
        lambda c: spread[c][2](),
        feed,
    )

    def f_step(stage, g, c):
        if stage == 0:
            down_product(g, c)
        elif stage == 3:
            finish(g, c)
        else:
            mlp[g * CHUNKS + c][stage]()

    def do(*words):
        for word in words:
            with jax.named_scope(word):
                kind, digits = word[0], [int(d) for d in word[1:] if d.isdigit()]
                if kind == "w":
                    w_steps[word[:2]](word[3:])
                elif kind == "t":
                    parts[digits[1]][digits[0] - 1]()
                elif kind == "p":
                    pack()
                elif kind == "n":
                    part_start(*digits)
                elif kind == "g":
                    part_end(*digits)
                elif kind == "m":
                    m_steps[digits[0]](digits[1])
                elif kind == "u":
                    unpack(*digits)
                else:
                    f_step(*digits)

    do("w1_rec", "w1_gate", "t10", "t11", "t12", "w1_out", "p", "w2_rec", "w2_gate", "t20", "w2_out", "w3_rec", "w3_gate", "t21")
    do("w4_rec", "w4_gate", "w3_out", "t22", "w6_rec", "w6_gate", "t30", "w4_out", "w6_out", "w1_up", "w1_d0", "t31", "t40", "n0")
    do("t32", "g0", "w5_out", "m00", "t41", "n1", "w2_up", "m10", "g1", "m01", "t42", "n2", "m20", "m11", "g2", "m02", "m03")
    do("m12", "m13", "m30", "w3_up", "w2_d0", "m21", "m22", "w4_up", "m31", "w6_up", "w1_d1", "m40", "m23", "m32", "w3_d0", "w4_d0")
    do("m50", "m41", "m33", "w5_up", "m60", "w2_d1", "m51", "m42", "w6_d0", "m61", "m43", "u00", "m52", "w3_d1", "m62", "m53")
    do("w4_d1", "w5_d0", "u01", "f000", "f001", "f100", "w6_d1", "m63", "f002", "f101", "f003", "f102", "f103", "u10", "f200", "f201")
    do("w5_d1", "u11", "f202", "f203", "f010", "f011", "f110", "f012", "f111", "f013", "f112", "f113", "f300", "f301", "f302", "f303")
    do("f210", "f211", "f212", "f213", "f310", "f311", "f312", "f313")

    with jax.named_scope("drain"):
        w_drain()
        landed(tok_all.at[pl.ds(0, 7)], ag_sent.at[0])
        landed(mid_all.at[pl.ds(0, 7)], ag_sent.at[1])
        for bufs in (m_bufs, f_bufs):
            _, from_core, half_sent, _, full_sent, _, _, sent = bufs
            landed(from_core, sent.at[0])
            landed(half_sent, sent.at[1])
            landed(full_sent, sent.at[2])


def shards(
    tokens,
    mixer_gain,
    rec_weight,
    gate_weight,
    conv_taps,
    recur_map,
    input_map,
    decay_param,
    out_weight,
    mlp_gain,
    up_weight,
    down_weight,
):
    hbm = pl.BlockSpec(memory_space=pl.ANY)

    def sums(count, width):
        shapes = [(2, 4, R, width), (4, R, width), (R, width), (R, width), (2, R, width), (2, R, width)]
        return [pltpu.VMEM((count, *shape), BF16) for shape in shapes]

    return pl.pallas_call(
        kernel,
        out_shape=pltpu.VMEM((TOK, CH), BF16),
        in_specs=[hbm] * 12,
        out_specs=pl.BlockSpec(memory_space=pltpu.VMEM),
        scratch_shapes=[
            pltpu.VMEM((1, D), F32),
            pltpu.VMEM((4, CH), BF16),
            pltpu.VMEM((1, CH, CH), BF16),
            pltpu.VMEM((1, CH, CH), BF16),
            pltpu.VMEM((1, CH), F32),
            pltpu.VMEM((1, D), F32),
            pltpu.VMEM((16, D // 16, CH), BF16),
            pltpu.VMEM((16, D // 16, CH), BF16),
            pltpu.VMEM((16, CH, D // 16), BF16),
            pltpu.VMEM((16, D // 16, FF), BF16),
            pltpu.VMEM((16, FF // 2, D // 16), BF16),
            pltpu.VMEM((16, FF // 2, D // 16), BF16),
            pltpu.VMEM((FF, D // 16), BF16),
            pltpu.VMEM((2, 4, FF, CH), BF16),
            pltpu.VMEM((8, TOK, CH), BF16),
            pltpu.VMEM((8, TOK, CH), BF16),
            pltpu.VMEM((TOK, D), BF16),
            pltpu.VMEM((TOK + 8, CH), F32),
            pltpu.VMEM((TOK, CH), F32),
            pltpu.VMEM((2, TOK, 128), F32),
            pltpu.VMEM((2, TOK, 128), F32),
            pltpu.VMEM((TOK, CH), BF16),
            pltpu.VMEM((TOK, FF), BF16),
            pltpu.VMEM((TOK, 128), F32),
            *sums(CHUNKS, CH),
            *sums(2 * CHUNKS, CH // 2),
            pltpu.SemaphoreType.DMA((12,)),
            pltpu.SemaphoreType.DMA((6, 5)),
            pltpu.SemaphoreType.DMA((6,)),
            pltpu.SemaphoreType.DMA((PARTS + CHUNKS, 3)),
            pltpu.SemaphoreType.DMA((2,)),
            pltpu.SemaphoreType.DMA((CHUNKS, 3)),
            pltpu.SemaphoreType.DMA((3,)),
            pltpu.SemaphoreType.DMA((2 * CHUNKS, 3)),
            pltpu.SemaphoreType.DMA((3,)),
        ],
        compiler_params=pltpu.CompilerParams(
            collective_id=0, has_side_effects=True, vmem_limit_bytes=60 * 1024 * 1024
        ),
    )(
        tokens,
        rec_weight,
        gate_weight,
        out_weight,
        up_weight,
        down_weight,
        mixer_gain.reshape(1, D),
        conv_taps,
        recur_map,
        input_map,
        decay_param.reshape(1, CH),
        mlp_gain.reshape(1, D),
    )


def solution(mesh):
    placed = (
        P(("rep", "fs"), "tp"),
        P(),
        P("fs", "tp"),
        P("fs", "tp"),
        P(None, "tp"),
        P("tp", None, None),
        P("tp", None, None),
        P("tp"),
        P("tp", "fs"),
        P(),
        P("fs", "tp"),
        P("tp", "fs"),
    )
    return jax.shard_map(
        shards, mesh=mesh, in_specs=placed, out_specs=P(("rep", "fs"), "tp"), check_vma=False
    )
```

time: 106 us -> 89 us (0.84)
  Pallas kernels: 104 us -> 88.2 us
    pallas_call x1, Pallas kernels: 104 us -> 88.2 us  [shards(): pl.pallas_call(kernel, out_shape=pltpu.VMEM((TOK, CH), BF16), in_specs=[h...]
where the time goes in v2:
time: 89 us; the launch traced here: 88.9 us
  Pallas kernels  88.2 us (99%)
    pallas_call x1, Pallas kernels, shards(): pl.pallas_call(kernel, out_shape=pltpu.VMEM((TOK, CH), BF16), in_specs=[h...  88.2 us

profile of v2, /device:TPU:1, one launch (start us, length us, event | category | flops | bytes accessed | tf_op | source)
XLA Modules:
  0.0 88.9 jit_solution(14575774036586955967)
XLA Ops:
  0.0 88.2 %shard_map.118 = bf16[768,256]{1,0:T(8,128)(2,1)S(1)} custom-call(bf16[768,256]{1,0:T(8,128)(2,1)} %tokens.1, bf16[128,256]{1,0:T(8,128)(2,1)} %rec_shard.1, bf16[128,256]{1,0:T(8,128)(2,1)} %gate_shard.1, bf16[256,128]{1,0:T(8,128)(2,1)} %out_shard.1, bf16[128,1024]{1,0:T(8,128)(2,1)} %up_shard.1, bf16[1024,128]{1,0:T(8,128)(2,1)} %down_shard.1, ...), custom_call_target="tpu_custom_call" | custom-call | tf_op jit(solution)/shard_map/pallas_call | solution.py:530
  88.2 0.7 copy.14

commit v3 on v2

--- a/solution.py
+++ b/solution.py
@@ -263,10 +263,10 @@
         return start, one, two, three
 
     def norm(buf, gain, first, count):
-        step = 64
+        step = count // 2
 
         def body(i, _):
-            rows = pl.ds(pl.multiple_of(first + i * step, step), step)
+            rows = pl.ds(pl.multiple_of(first + i * step, 32), step)
             total = jnp.zeros((step, CH), F32)
             for j in range(8):
                 v = buf[j, rows, :].astype(F32)
@@ -357,11 +357,11 @@
         return lax.broadcasted_iota(jnp.int32, shape, 1) < 64
 
     def pack():
-        step = 128
+        step, odd = 128, lax.rem(x, 2)
 
         def body(i, _):
-            upper = down_raw[pl.ds(pl.multiple_of(i * step, step), step), :].astype(F32)
-            lower = down_raw[pl.ds(pl.multiple_of(i * step + FF // 2, step), step), :].astype(F32)
+            upper = down_raw[pl.ds(pl.multiple_of(i * step + odd * (FF // 2), step), step), :].astype(F32)
+            lower = down_raw[pl.ds(pl.multiple_of(i * step + (1 - odd) * (FF // 2), step), step), :].astype(F32)
             low = low_lanes((step, 128))
             rows = pl.ds(pl.multiple_of(i * step, step), step)
             w_d0[z * 4 + x, rows, :] = jnp.where(low, upper, pltpu.roll(lower, 64, 1)).astype(BF16)
@@ -375,10 +375,11 @@
         low = low_lanes((128, 128))
         cols = pl.ds(pl.multiple_of(128 * side, 128), 128)
         for k in range(step // 128):
-            left = w[4 * n + 2 * side, pl.ds(first + 128 * k, 128), :].astype(F32)
-            right = w[4 * n + 2 * side + 1, pl.ds(first + 128 * k, 128), :].astype(F32)
-            w_dn[g, n, pl.ds(first + 128 * k, 128), cols] = jnp.where(low, left, pltpu.roll(right, 64, 1)).astype(BF16)
-            w_dn[g, n, pl.ds(first + FF // 2 + 128 * k, 128), cols] = jnp.where(low, pltpu.roll(left, 64, 1), right).astype(BF16)
+            left = w[4 * n + 2 * side, pl.ds(first + 128 * k, 128), :]
+            right = w[4 * n + 2 * side + 1, pl.ds(first + 128 * k, 128), :]
+            w_dn[g, n, pl.ds(first + 128 * k, 128), cols] = jnp.where(low, left, right)
+            swapped = jnp.where(low, right, left).astype(F32)
+            w_dn[g, n, pl.ds(first + FF // 2 + 128 * k, 128), cols] = pltpu.roll(swapped, 64, 1).astype(BF16)
 
     def unpack(g, late):
         pair = lax.div(x, 2)
@@ -437,7 +438,6 @@
     w_steps = {"w1": w1, "w2": w2, "w3": w3, "w4": w4, "w5": w5, "w6": w6}
 
     def part_start(m):
-        norm(tok_all, mixer_gain, m * PART, PART)
         if m == 0:
             padded[pl.ds(0, 8), :] = jnp.zeros((8, CH), F32)
             w5("rec")
@@ -476,6 +476,8 @@
                     parts[digits[1]][digits[0] - 1]()
                 elif kind == "p":
                     pack()
+                elif kind == "a":
+                    norm(tok_all, mixer_gain, digits[0] * PART, PART)
                 elif kind == "n":
                     part_start(*digits)
                 elif kind == "g":
@@ -488,13 +490,13 @@
                     f_step(*digits)
 
     do("w1_rec", "w1_gate", "t10", "t11", "t12", "w1_out", "p", "w2_rec", "w2_gate", "t20", "w2_out", "w3_rec", "w3_gate", "t21")
-    do("w4_rec", "w4_gate", "w3_out", "t22", "w6_rec", "w6_gate", "t30", "w4_out", "w6_out", "w1_up", "w1_d0", "t31", "t40", "n0")
-    do("t32", "g0", "w5_out", "m00", "t41", "n1", "w2_up", "m10", "g1", "m01", "t42", "n2", "m20", "m11", "g2", "m02", "m03")
-    do("m12", "m13", "m30", "w3_up", "w2_d0", "m21", "m22", "w4_up", "m31", "w6_up", "w1_d1", "m40", "m23", "m32", "w3_d0", "w4_d0")
-    do("m50", "m41", "m33", "w5_up", "m60", "w2_d1", "m51", "m42", "w6_d0", "m61", "m43", "u00", "m52", "w3_d1", "m62", "m53")
-    do("w4_d1", "w5_d0", "u01", "f000", "f001", "f100", "w6_d1", "m63", "f002", "f101", "f003", "f102", "f103", "u10", "f200", "f201")
-    do("w5_d1", "u11", "f202", "f203", "f010", "f011", "f110", "f012", "f111", "f013", "f112", "f113", "f300", "f301", "f302", "f303")
-    do("f210", "f211", "f212", "f213", "f310", "f311", "f312", "f313")
+    do("w4_rec", "w4_gate", "w3_out", "t22", "w6_rec", "w6_gate", "t30", "w4_out", "t31", "t40", "a0", "w6_out", "w1_up", "w1_d0")
+    do("t41", "a1", "n0", "t32", "g0", "w5_out", "m00", "n1", "w2_up", "m10", "g1", "m01", "t42", "a2", "n2", "m20", "m11", "g2")
+    do("m02", "m03", "m12", "m13", "m30", "w3_up", "w2_d0", "m21", "m22", "w4_up", "m31", "w6_up", "w3_d0", "w1_d1", "m40", "m23")
+    do("w4_d0", "m32", "m50", "m41", "m33", "w5_up", "m60", "w6_d0", "w2_d1", "m51", "m42", "m61", "m43", "u00", "w3_d1", "m52")
+    do("w5_d0", "u01", "f000", "f001", "f100", "w4_d1", "m53", "m62", "w6_d1", "f101", "f002", "m63", "f102", "f003", "f200", "f201")
+    do("u10", "f103", "w5_d1", "u11", "f010", "f011", "f202", "f110", "f012", "f203", "f111", "f013", "f112", "f113", "f300", "f301")
+    do("f210", "f302", "f211", "f303", "f212", "f213", "f310", "f311", "f312", "f313")
 
     with jax.named_scope("drain"):
         w_drain()

time: 89 us -> 86.9 us (0.976)
  Pallas kernels: 88.2 us -> 86 us
    pallas_call x1, Pallas kernels: 88.2 us -> 86 us  [shards(): pl.pallas_call(kernel, out_shape=pltpu.VMEM((TOK, CH), BF16), in_specs=[h...]
where the time goes in v3:
time: 86.9 us; the launch traced here: 86.8 us
  Pallas kernels  86 us (99%)
    pallas_call x1, Pallas kernels, shards(): pl.pallas_call(kernel, out_shape=pltpu.VMEM((TOK, CH), BF16), in_specs=[h...  86 us

profile of v3, /device:TPU:1, one launch (start us, length us, event | category | flops | bytes accessed | tf_op | source)
XLA Modules:
  0.0 86.8 jit_solution(5114159694461112948)
XLA Ops:
  0.0 86.0 %shard_map.118 = bf16[768,256]{1,0:T(8,128)(2,1)S(1)} custom-call(bf16[768,256]{1,0:T(8,128)(2,1)} %tokens.1, bf16[128,256]{1,0:T(8,128)(2,1)} %rec_shard.1, bf16[128,256]{1,0:T(8,128)(2,1)} %gate_shard.1, bf16[256,128]{1,0:T(8,128)(2,1)} %out_shard.1, bf16[128,1024]{1,0:T(8,128)(2,1)} %up_shard.1, bf16[1024,128]{1,0:T(8,128)(2,1)} %down_shard.1, ...), custom_call_target="tpu_custom_call" | custom-call | tf_op jit(solution)/shard_map/pallas_call | solution.py:532
  86.0 0.7 copy.14

commit v4 on v3

--- a/solution.py
+++ b/solution.py
@@ -233,23 +233,27 @@
         return one, two, three, four
 
     top, bottom = pl.ds(0, H), pl.ds(H, H)
+    leaving = (y2, yp, ym, y)
 
     def rs(k, part, from_core, half_sent, half_got, full_sent, full_got, sems, sent):
         sem = lambda n: sems.at[k, n]
         both = lambda n: part[k, core, n].astype(F32) + from_core[k, n].astype(F32)
 
-        def start():
-            send(part.at[k, other], from_core.at[k], sent.at[0], sem(0), partner)
+        def first():
+            send(part.at[k, other, 0], from_core.at[k, 0], sent.at[0], sem(0), partner)
+
+        def rest():
+            send(part.at[k, other, pl.ds(1, 3)], from_core.at[k, pl.ds(1, 3)], sent.at[0], sem(1), partner)
 
         def one():
-            landed(from_core.at[k], sem(0))
-            half_sent[k] = both(y2).astype(BF16)
+            landed(from_core.at[k, 0], sem(0))
+            half_sent[k] = both(0).astype(BF16)
             send(half_sent.at[k, top], half_got.at[k, top], sent.at[1], sem(1), y_up)
             send(half_sent.at[k, bottom], half_got.at[k, bottom], sent.at[1], sem(1), y_down)
 
         def two():
-            landed(half_got.at[k], sem(1))
-            up, down = both(yp), both(ym)
+            landed(from_core.at[k], sem(1))
+            up, down = both(1), both(2)
             got = half_got[k].astype(F32)
             full_sent[k, 0] = jnp.concatenate([up[:H] + got[:H], up[H:]], axis=0).astype(BF16)
             send(full_sent.at[k, 0], full_got.at[k, 0], sent.at[2], sem(2), y_up)
@@ -258,9 +262,9 @@
 
         def three():
             landed(full_got.at[k], sem(2))
-            return both(y) + (full_got[k, 0].astype(F32) + full_got[k, 1].astype(F32))
-
-        return start, one, two, three
+            return both(3) + (full_got[k, 0].astype(F32) + full_got[k, 1].astype(F32))
+
+        return first, one, two, three, rest
 
     def norm(buf, gain, first, count):
         step = count // 2
@@ -339,12 +343,18 @@
 
     def out_product(c):
         lhs = mixed[pl.ds(c * R, R), :]
-        for side in (other, core):
-            for n in range(4):
-                rhs = jnp.concatenate([w_out[4 * n + 2 * side], w_out[4 * n + 2 * side + 1]], axis=1)
-                m_part[c, side, n] = jnp.dot(lhs, rhs, preferred_element_type=F32).astype(BF16)
-            if side is other:
-                mixer[c][0]()
+
+        def term(r, side):
+            place = 4 * leaving[r] + 2 * side
+            rhs = jnp.concatenate([w_out[place], w_out[place + 1]], axis=1)
+            m_part[c, side, r] = jnp.dot(lhs, rhs, preferred_element_type=F32).astype(BF16)
+
+        for r in range(4):
+            term(r, other)
+        mixer[c][0]()
+        mixer[c][4]()
+        for r in range(4):
+            term(r, core)
 
     def lift(c):
         lhs = normed[pl.ds(c * R, R), :]
@@ -396,14 +406,13 @@
             for side in range(2):
                 unpack_rows(g, n, side, 0)
 
-    def down_product(g, c):
+    def down_product(g, c, terms):
         k = g * CHUNKS + c
         lhs = squared[pl.ds(c * R, R), :]
-        for n in range(4):
-            product = jnp.dot(lhs, w_dn[g, n], preferred_element_type=F32).astype(BF16)
-            f_part[k, 0, n] = product[:, :128]
-            f_part[k, 1, n] = product[:, 128:]
-        mlp[k][0]()
+        for r in terms:
+            product = jnp.dot(lhs, w_dn[g, leaving[r]], preferred_element_type=F32).astype(BF16)
+            f_part[k, 0, r] = product[:, :128]
+            f_part[k, 1, r] = product[:, 128:]
 
     parts = [ag(n, tok_all, n * PART, PART, ag_sent.at[0]) for n in range(PARTS)]
     spread = [ag(PARTS + c, mid_all, c * R, R, ag_sent.at[1]) for c in range(CHUNKS)]
@@ -460,7 +469,17 @@
 
     def f_step(stage, g, c):
         if stage == 0:
-            down_product(g, c)
+            down_product(g, c, (0, 1, 2, 3))
+            mlp[g * CHUNKS + c][0]()
+            mlp[g * CHUNKS + c][4]()
+        elif stage == 5:
+            for n in range(CHUNKS):
+                down_product(g, n, (0,))
+            for n in range(CHUNKS):
+                mlp[g * CHUNKS + n][0]()
+        elif stage == 4:
+            down_product(g, c, (1, 2, 3))
+            mlp[g * CHUNKS + c][4]()
         elif stage == 3:
             finish(g, c)
         else:
@@ -491,12 +510,12 @@
 
     do("w1_rec", "w1_gate", "t10", "t11", "t12", "w1_out", "p", "w2_rec", "w2_gate", "t20", "w2_out", "w3_rec", "w3_gate", "t21")
     do("w4_rec", "w4_gate", "w3_out", "t22", "w6_rec", "w6_gate", "t30", "w4_out", "t31", "t40", "a0", "w6_out", "w1_up", "w1_d0")
-    do("t41", "a1", "n0", "t32", "g0", "w5_out", "m00", "n1", "w2_up", "m10", "g1", "m01", "t42", "a2", "n2", "m20", "m11", "g2")
-    do("m02", "m03", "m12", "m13", "m30", "w3_up", "w2_d0", "m21", "m22", "w4_up", "m31", "w6_up", "w3_d0", "w1_d1", "m40", "m23")
-    do("w4_d0", "m32", "m50", "m41", "m33", "w5_up", "m60", "w6_d0", "w2_d1", "m51", "m42", "m61", "m43", "u00", "w3_d1", "m52")
-    do("w5_d0", "u01", "f000", "f001", "f100", "w4_d1", "m53", "m62", "w6_d1", "f101", "f002", "m63", "f102", "f003", "f200", "f201")
-    do("u10", "f103", "w5_d1", "u11", "f010", "f011", "f202", "f110", "f012", "f203", "f111", "f013", "f112", "f113", "f300", "f301")
-    do("f210", "f302", "f211", "f303", "f212", "f213", "f310", "f311", "f312", "f313")
+    do("t41", "a1", "n0", "t32", "g0", "w5_out", "m00", "n1", "m10", "g1", "w2_up", "m01", "t42", "a2", "n2", "m20", "m11", "g2")
+    do("m02", "m03", "m12", "m13", "m30", "w3_up", "w2_d0", "m21", "m22", "m23", "w4_up", "m40", "m31", "w6_up", "w3_d0", "w1_d1")
+    do("m32", "w4_d0", "m33", "m50", "m41", "w5_up", "m60", "m42", "w6_d0", "w2_d1", "m43", "m51", "u00", "m52", "m61", "m53")
+    do("m62", "w3_d1", "w5_d0", "u01", "m63", "w4_d1", "f000", "f001", "f100", "w6_d1", "f002", "f101", "f003", "f102", "u10", "f103")
+    do("f200", "f201", "w5_d1", "u11", "f510", "f410", "f202", "f110", "f111", "f411", "f112", "f113", "f203", "f412", "f413", "f300")
+    do("f210", "f211", "f212", "f301", "f213", "f302", "f303", "f310", "f311", "f312", "f313")
 
     with jax.named_scope("drain"):
         w_drain()

time: 86.9 us -> 86.5 us (level)
  no operation moved by 1% of the time
where the time goes in v4:
time: 86.5 us; the launch traced here: 86.4 us
  Pallas kernels  85.7 us (99%)
    pallas_call x1, Pallas kernels, shards(): pl.pallas_call(kernel, out_shape=pltpu.VMEM((TOK, CH), BF16), in_specs=[h...  85.7 us

profile of v4, /device:TPU:1, one launch (start us, length us, event | category | flops | bytes accessed | tf_op | source)
XLA Modules:
  0.0 86.4 jit_solution(11054016817714709022)
XLA Ops:
  0.0 85.7 %shard_map.118 = bf16[768,256]{1,0:T(8,128)(2,1)S(1)} custom-call(bf16[768,256]{1,0:T(8,128)(2,1)} %tokens.1, bf16[128,256]{1,0:T(8,128)(2,1)} %rec_shard.1, bf16[128,256]{1,0:T(8,128)(2,1)} %gate_shard.1, bf16[256,128]{1,0:T(8,128)(2,1)} %out_shard.1, bf16[128,1024]{1,0:T(8,128)(2,1)} %up_shard.1, bf16[1024,128]{1,0:T(8,128)(2,1)} %down_shard.1, ...), custom_call_target="tpu_custom_call" | custom-call | tf_op jit(solution)/shard_map/pallas_call | solution.py:551
  85.7 0.7 copy.14

commit v5 on v4

--- a/solution.py
+++ b/solution.py
@@ -573,8 +573,8 @@
             pltpu.VMEM((TOK, D), BF16),
             pltpu.VMEM((TOK + 8, CH), F32),
             pltpu.VMEM((TOK, CH), F32),
-            pltpu.VMEM((2, TOK, 128), F32),
-            pltpu.VMEM((2, TOK, 128), F32),
+            pltpu.VMEM((2, TOK + SEG, 128), F32),
+            pltpu.VMEM((2, TOK + SEG, 128), F32),
             pltpu.VMEM((TOK, CH), BF16),
             pltpu.VMEM((TOK, FF), BF16),
             pltpu.VMEM((TOK, 128), F32),

time: 86.5 us -> 86.5 us (level)
  no operation moved by 1% of the time
where the time goes in v5:
time: 86.5 us; the launch traced here: 86.4 us
  Pallas kernels  85.7 us (99%)
    pallas_call x1, Pallas kernels, shards(): pl.pallas_call(kernel, out_shape=pltpu.VMEM((TOK, CH), BF16), in_specs=[h...  85.7 us

profile of v5, /device:TPU:1, one launch (start us, length us, event | category | flops | bytes accessed | tf_op | source)
XLA Modules:
  0.0 86.4 jit_solution(14226658096649881239)
XLA Ops:
  0.0 85.7 %shard_map.118 = bf16[768,256]{1,0:T(8,128)(2,1)S(1)} custom-call(bf16[768,256]{1,0:T(8,128)(2,1)} %tokens.1, bf16[128,256]{1,0:T(8,128)(2,1)} %rec_shard.1, bf16[128,256]{1,0:T(8,128)(2,1)} %gate_shard.1, bf16[256,128]{1,0:T(8,128)(2,1)} %out_shard.1, bf16[128,1024]{1,0:T(8,128)(2,1)} %up_shard.1, bf16[1024,128]{1,0:T(8,128)(2,1)} %down_shard.1, ...), custom_call_target="tpu_custom_call" | custom-call | tf_op jit(solution)/shard_map/pallas_call | solution.py:551
  85.7 0.7 copy.14
